TPU v7x, 32 devices: a whole 2x2x4 slice. The times are simulated.
32 devices in a mesh: grp: 2 (over y), fs: 4 (over z), tp: 4 (over x, core).
Axes of the slice: x: 2, y: 2, z: 4, core: 2. Of those that a mesh axis runs over, the one named last changes fastest.
Arguments:
- tokens: bfloat16 [4096, 2048], P(('grp', 'fs', 'tp')), parts along dimension 0, may hold values from -6 to 6
- route_ids: int32 [4096, 8], P(('grp', 'fs', 'tp')), parts along dimension 0, may hold values from 0 to 15, all different within a row; in each aligned block of 128 rows (0 to 127, 128 to 255, ...) at most 96 rows name the same one
- route_scores: float32 [4096, 8], P(('grp', 'fs', 'tp')), parts along dimension 0, may hold values from 0.05 to 1
- norm_gain: float32 [2048], P('fs'), may hold values from 0.1 to 1.9
- expert_gate: float32 [16, 2048, 256], P(None, 'fs', 'tp'), may hold values from -0.125 to 0.125
- expert_up: float32 [16, 2048, 256], P(None, 'fs', 'tp'), may hold values from -0.125 to 0.125
- expert_down: float32 [16, 256, 2048], P(None, 'fs', 'tp'), may hold values from -0.375 to 0.375
- shared_gate: float32 [2048, 256], P('fs', 'tp'), may hold values from -0.125 to 0.125
- shared_up: float32 [2048, 256], P('fs', 'tp'), may hold values from -0.125 to 0.125
- shared_down: float32 [256, 2048], P('fs', 'tp'), may hold values from -0.375 to 0.375
Outputs:
- mixed: bfloat16 [4096, 2048], P(('grp', 'fs', 'tp')), parts along dimension 0
- sampler_gate: bfloat16 [32, 2048, 256], P(('grp', 'fs', 'tp')), parts along dimension 0
- sampler_up: bfloat16 [32, 2048, 256], P(('grp', 'fs', 'tp')), parts along dimension 0
- sampler_down: bfloat16 [32, 256, 2048], P(('grp', 'fs', 'tp')), parts along dimension 0
- sampler_shared_gate: bfloat16 [4096, 256], P(('grp', 'fs')), parts along dimension 0
- sampler_shared_up: bfloat16 [4096, 256], P(('grp', 'fs')), parts along dimension 0
- sampler_shared_down: bfloat16 [512, 2048], P(('grp', 'fs')), parts along dimension 0
There are 2 independent parts, one for each index of `grp`. A program takes and returns all parts, laid end to end along the dimension named above; an argument that names none is the same for every part. Nothing has to cross between parts.
Inputs may be any that keep to these rules, and one draw needn't show every extreme that they name: `route_ids`: each row names 8 different experts. Among the 128 rows of one device no expert is named more than 96 times, a bound that some block reaches.
All inputs are finite; a program needn't handle non-finite values.
Results may differ from a plain program's by a relative error of at most 0.0084.
Values may be sent and summed in bfloat16 or wider, within the bound.
A program may use at most 128 MiB of HBM per device.

v0:
```python
import jax
import jax.numpy as jnp
from jax import lax
from jax.sharding import PartitionSpec as P

EPSILON = 1e-06
route_scale = 2.5


def expert_rows(row_block, w_gate, w_up, w_down):
    gate_rows = jnp.dot(row_block, w_gate, preferred_element_type=jnp.float32)
    up_rows = jnp.dot(row_block, w_up, preferred_element_type=jnp.float32)
    hidden = (jax.nn.silu(gate_rows) * up_rows).astype(jnp.bfloat16)
    return jnp.dot(hidden, w_down, preferred_element_type=jnp.float32).astype(jnp.bfloat16)


def relayout(arrived, fs_count, tp_count):
    tile_rows = arrived.shape[2]
    tile_cols = arrived.shape[3]
    grid = arrived.reshape(fs_count, tp_count, tile_rows, tile_cols)
    grid = jnp.transpose(grid, (0, 2, 1, 3))
    return grid.reshape(1, fs_count * tile_rows, tp_count * tile_cols)


def on_device(
    tokens,
    route_ids,
    route_scores,
    norm_gain,
    expert_gate,
    expert_up,
    expert_down,
    shared_gate,
    shared_up,
    shared_down,
):
    fs_count = lax.axis_size("fs")
    tp_count = lax.axis_size("tp")
    experts = fs_count * tp_count
    gain_col = norm_gain[:, None]
    piece_gate = (gain_col[None] * expert_gate).astype(jnp.bfloat16)
    piece_up = (gain_col[None] * expert_up).astype(jnp.bfloat16)
    piece_down = expert_down.astype(jnp.bfloat16)
    moved = (
        lax.all_to_all(piece_gate[:, None], ("fs", "tp"), split_axis=0, concat_axis=1, tiled=True),
        lax.all_to_all(piece_up[:, None], ("fs", "tp"), split_axis=0, concat_axis=1, tiled=True),
        lax.all_to_all(piece_down[:, None], ("fs", "tp"), split_axis=0, concat_axis=1, tiled=True),
    )
    served_gate = relayout(moved[0], fs_count, tp_count)
    served_up = relayout(moved[1], fs_count, tp_count)
    served_down = relayout(moved[2], fs_count, tp_count)
    tile_gate = (gain_col * shared_gate).astype(jnp.bfloat16)
    tile_up = (gain_col * shared_up).astype(jnp.bfloat16)
    tile_down = shared_down.astype(jnp.bfloat16)
    held_gate, held_up, held_down = (
        lax.all_gather(tile_gate, "tp", axis=1, tiled=True),
        lax.all_gather(tile_up, "tp", axis=1, tiled=True),
        lax.all_gather(tile_down, "tp", axis=1, tiled=True),
    )
    rows_dev = tokens.shape[0]
    width = tokens.shape[1]
    picks = route_ids.shape[1]
    capacity = 3 * rows_dev * picks // (2 * experts)
    widened = tokens.astype(jnp.float32)
    normed = (
        widened * lax.rsqrt(jnp.mean(widened * widened, axis=1, keepdims=True) + EPSILON)
    ).astype(jnp.bfloat16)
    weights = route_scale * route_scores / jnp.sum(route_scores, axis=1, keepdims=True)
    flat_ids = route_ids.reshape(-1)
    onehot = (flat_ids[:, None] == jnp.arange(experts, dtype=jnp.int32)[None, :]).astype(jnp.int32)
    earlier = jnp.cumsum(onehot, axis=0) - onehot
    ranks = jnp.sum(earlier * onehot, axis=1)
    target = flat_ids * capacity + ranks
    outbox = (
        jnp.zeros((experts * capacity, width), jnp.bfloat16)
        .at[target]
        .set(jnp.repeat(normed, picks, axis=0))
    )
    arrived = lax.all_to_all(
        outbox.reshape(experts, capacity, width),
        ("fs", "tp"),
        split_axis=0,
        concat_axis=0,
        tiled=True,
    )
    finished = expert_rows(
        arrived.reshape(-1, width), served_gate[0], served_up[0], served_down[0]
    ).reshape(arrived.shape)
    returned = lax.all_to_all(finished, ("fs", "tp"), split_axis=0, concat_axis=0, tiled=True)
    results = returned.reshape(experts * capacity, width)[target]
    routed = jnp.sum(
        results.reshape(rows_dev, picks, width).astype(jnp.float32) * weights[:, :, None], axis=1
    )
    columns = normed
    gate_part = jnp.dot(
        columns,
        lax.all_gather(held_gate, "fs", axis=0, tiled=True),
        preferred_element_type=jnp.float32,
    )
    up_part = jnp.dot(
        columns,
        lax.all_gather(held_up, "fs", axis=0, tiled=True),
        preferred_element_type=jnp.float32,
    )
    shared_hidden = (jax.nn.silu(gate_part) * up_part).astype(jnp.bfloat16)
    columns = shared_hidden
    shared_term = jnp.dot(
        columns,
        lax.all_gather(held_down, "fs", axis=0, tiled=True),
        preferred_element_type=jnp.float32,
    )
    mixed = (routed + shared_term).astype(jnp.bfloat16)
    return (mixed, served_gate, served_up, served_down, held_gate, held_up, held_down)


def solution(mesh):
    return jax.shard_map(
        on_device,
        mesh=mesh,
        in_specs=(
            P(("grp", "fs", "tp"), None),
            P(("grp", "fs", "tp"), None),
            P(("grp", "fs", "tp"), None),
            P("fs"),
            P(None, "fs", "tp"),
            P(None, "fs", "tp"),
            P(None, "fs", "tp"),
            P("fs", "tp"),
            P("fs", "tp"),
            P("fs", "tp"),
        ),
        out_specs=(
            P(("grp", "fs", "tp"), None),
            P(("grp", "fs", "tp"), None, None),
            P(("grp", "fs", "tp"), None, None),
            P(("grp", "fs", "tp"), None, None),
            P(("grp", "fs"), None),
            P(("grp", "fs"), None),
            P(("grp", "fs"), None),
        ),
        check_vma=False,
    )
```

profile of v0, /device:TPU:11, one launch (start us, length us, event | category | flops | bytes accessed | tf_op | source)
XLA Modules:
  0.0 485.5 jit_solution(11063605218181208656)
XLA Ops:
  7.2 3.8 fusion.10
  11.0 31.1 %all_to_all.37 = bf16[16,1,512,64]{2,3,1,0:T(8,128)(2,1)S(1)} all-to-all(bf16[16,1,512,64]{2,3,1,0:T(8,128)(2,1)S(1)} %get-tuple-element.36), channel_id=1, replica_groups=mesh['grp'=2,'fs'=4,'tp'=4] {'fs','tp'}, dimensions={0} | all-to-all | bytes 2097152 | tf_op jit(solution)/shard_map/all_to_all | solution.py:45
  42.1 5.0 %all-to-all-start.2 = ((bf16[16,1,512,64]{2,3,1,0:T(8,128)(2,1)}), bf16[16,1,512,64]{2,3,1,0:T(8,128)(2,1)S(1)}, u32[]{:S(2)}, u32[]{:S(2)}) async-start(bf16[16,1,512,64]{2,3,1,0:T(8,128)(2,1)} %get-tuple-element.37), calls=%async_computation.2 | async-start | bytes 2097152 | tf_op jit(solution)/shard_map/all_to_all | solution.py:46
  47.1 2.7 convert_bitcast_fusion
  49.9 22.1 %all-to-all-done.2 = bf16[16,1,512,64]{2,3,1,0:T(8,128)(2,1)S(1)} async-done(((bf16[16,1,512,64]{2,3,1,0:T(8,128)(2,1)}), bf16[16,1,512,64]{2,3,1,0:T(8,128)(2,1)S(1)}, u32[]{:S(2)}, u32[]{:S(2)}) %all-to-all-start.2) | async-done | bytes 1048608 | tf_op jit(solution)/shard_map/all_to_all | solution.py:46
  72.0 4.8 all-to-all-start.3
  77.1 4.5 reduce-window.6
  82.7 10.2 %scatter_custom_fusion = bf16[1536,2048]{1,0:T(8,128)(2,1)} fusion(s32[1024]{0:T(1024)S(1)} %bitcast.93, bf16[]{:T(256)} %constant.9.clone.1, bf16[128,2048]{1,0:T(8,128)(2,1)S(1)} %fusion.9), kind=kCustom, calls=%fused_computation.5 | custom fusion | bytes 6815746 | tf_op jit(solution)/shard_map/scatter | solution.py:77
  92.9 8.9 %all-to-all-done.3 = bf16[16,1,64,512]{3,2,1,0:T(8,128)(2,1)} async-done(((bf16[16,1,64,512]{3,2,1,0:T(8,128)(2,1)}), bf16[16,1,64,512]{3,2,1,0:T(8,128)(2,1)}, u32[]{:S(2)}, u32[]{:S(2)}) %all-to-all-start.3) | async-done | bytes 1048608 | tf_op jit(solution)/shard_map/all_to_all | solution.py:47
  101.8 4.8 all-to-all-start
  107.4 1.2 copy.67
  110.8 2.0 copy.77
  112.8 1.2 copy.69
  114.0 130.0 %all-to-all-done = bf16[16,96,2048]{2,1,0:T(8,128)(2,1)} async-done(((bf16[16,96,2048]{2,1,0:T(8,128)(2,1)}), bf16[16,96,2048]{2,1,0:T(8,128)(2,1)}, u32[]{:S(2)}, u32[]{:S(2)}) %all-to-all-start) | async-done | bytes 6291488 | tf_op jit(solution)/shard_map/all_to_all | solution.py:79
  244.0 6.1 %fusion.25 = f32[1536,256]{1,0:T(8,128)} fusion(bf16[1536,2048]{1,0:T(8,128)(2,1)} %bitcast.6, bf16[2048,256]{0,1:T(8,128)(2,1)} %bitcast.87), kind=kOutput, calls=%fused_computation.51 | convolution fusion | flops 1610612736 | bytes 8912896 | tf_op jit(solution)/shard_map/dot_general | solution.py:11
  250.1 12.9 %convolution_convert_fusion = bf16[1536,2048]{1,0:T(8,128)(2,1)} fusion(bf16[256,2048]{1,0:T(8,128)(2,1)} %bitcast.89, bf16[1536,2048]{1,0:T(8,128)(2,1)} %bitcast.6, bf16[2048,256]{0,1:T(8,128)(2,1)} %bitcast.88, f32[1536,256]{1,0:T(8,128)} %fusion.25), kind=kOutput, calls=%fused_computation.4 | convolution fusion | flops 3226730496 | bytes 16252928 | tf_op jit(solution)/shard_map/dot_general | solution.py:14
  263.0 4.9 %all-to-all-start.4 = ((bf16[16,96,2048]{2,1,0:T(8,128)(2,1)}), bf16[16,96,2048]{2,1,0:T(8,128)(2,1)}, u32[]{:S(2)}, u32[]{:S(2)}) async-start(bf16[16,96,2048]{2,1,0:T(8,128)(2,1)} %bitcast.84), calls=%async_computation.4 | async-start | bytes 12582912 | tf_op jit(solution)/shard_map/all_to_all | solution.py:89
  268.0 29.8 %all_gather.18 = bf16[512,256]{0,1:T(8,128)(2,1)} all-gather(bf16[512,64]{0,1:T(8,128)(2,1)S(1)} %get-tuple-element.34), channel_id=1, replica_groups=mesh['grp'=2,'fs'=4,'tp'=4] {'tp'}, dimensions={1}, use_global_device_ids=true | all-gather | bytes 327680 | tf_op jit(solution)/shard_map/all_gather | solution.py:56
  298.0 10.4 %all_gather.20 = bf16[512,256]{0,1:T(8,128)(2,1)} all-gather(bf16[512,64]{0,1:T(8,128)(2,1)S(1)} %get-tuple-element.35), channel_id=1, replica_groups=mesh['grp'=2,'fs'=4,'tp'=4] {'tp'}, dimensions={1}, use_global_device_ids=true | all-gather | bytes 327680 | tf_op jit(solution)/shard_map/all_gather | solution.py:57
  309.3 8.1 %all_gather.22 = bf16[64,2048]{1,0:T(8,128)(2,1)} all-gather(bf16[64,512]{1,0:T(8,128)(2,1)S(1)} %convert_element_type.63), channel_id=1, replica_groups=mesh['grp'=2,'fs'=4,'tp'=4] {'tp'}, dimensions={1}, use_global_device_ids=true | all-gather | bytes 327680 | tf_op jit(solution)/shard_map/all_gather | solution.py:58
  317.4 1.8 copy.64
  319.2 1.8 copy.65
  321.1 52.7 %all-gather.4.cloned.1.call-done = bf16[2048,256]{0,1:T(8,128)(2,1)} async-done(((bf16[512,256]{0,1:T(8,128)(2,1)}), bf16[2048,256]{0,1:T(8,128)(2,1)}) %all-gather.4.cloned.1.call-update) | async-done | bytes 1048592 | tf_op jit(solution)/shard_map/all_gather | solution.py:97
  373.8 1.9 fusion.26
  375.7 1.6 reshape.129
  377.3 2.3 copy.62
  380.3 1.3 copy.63
  381.6 1.6 reshape.131
  383.2 72.7 %all-to-all-done.4 = bf16[16,96,2048]{2,1,0:T(8,128)(2,1)} async-done(((bf16[16,96,2048]{2,1,0:T(8,128)(2,1)}), bf16[16,96,2048]{2,1,0:T(8,128)(2,1)}, u32[]{:S(2)}, u32[]{:S(2)}) %all-to-all-start.4) | async-done | bytes 6291488 | tf_op jit(solution)/shard_map/all_to_all | solution.py:89
  455.9 12.4 %gather_fusion = bf16[1024,2048]{1,0:T(8,128)(2,1)} fusion(bf16[1536,2048]{1,0:T(8,128)(2,1)} %bitcast.18, s32[1024]{0:T(1024)S(1)} %broadcast_clamp_fusion), kind=kCustom, calls=%fused_computation | custom fusion | bytes 8392704 | tf_op jit(solution)/shard_map/gather | solution.py:90
  468.4 6.5 %fusion = f32[128,2048]{1,0:T(8,128)S(1)} fusion(bf16[1024,2048]{1,0:T(8,128)(2,1)} %gather_fusion, f32[128,8]{1,0:T(8,128)S(1)} %copy.61), kind=kLoop, calls=%fused_computation.3 | loop fusion | flops 6029312 | bytes 5246976 | tf_op jit(solution)/shard_map/reduce_sum | solution.py:91
  475.0 3.3 fusion.5
  (55 shorter events, 7.0 us)
Async XLA Ops:
  42.1 34.7 %copy-start.6 = (s32[128,8]{0,1:T(8,128)S(1)}, s32[128,8]{0,1:T(8,128)}, u32[]{:S(2)}) copy-start(s32[128,8]{0,1:T(8,128)} %param.11) | copy-start | bytes 12292
  42.1 40.2 %copy-start.3 = (bf16[128,2048]{1,0:T(8,128)(2,1)S(1)}, bf16[128,2048]{1,0:T(8,128)(2,1)}, u32[]{:S(2)}) copy-start(bf16[128,2048]{1,0:T(8,128)(2,1)} %param.10) | copy-start | bytes 1572868
  42.1 29.9 %all-to-all-start.2 = ((bf16[16,1,512,64]{2,3,1,0:T(8,128)(2,1)}), bf16[16,1,512,64]{2,3,1,0:T(8,128)(2,1)S(1)}, u32[]{:S(2)}, u32[]{:S(2)}) async-start(bf16[16,1,512,64]{2,3,1,0:T(8,128)(2,1)} %get-tuple-element.37), calls=%async_computation.2 | async-start | bytes 2097152 | tf_op jit(solution)/shard_map/all_to_all | solution.py:46
  72.0 29.8 %all-to-all-start.3 = ((bf16[16,1,64,512]{3,2,1,0:T(8,128)(2,1)}), bf16[16,1,64,512]{3,2,1,0:T(8,128)(2,1)}, u32[]{:S(2)}, u32[]{:S(2)}) async-start(bf16[16,1,64,512]{3,2,1,0:T(8,128)(2,1)} %convert_bitcast_fusion), calls=%async_computation.3 | async-start | bytes 2097152 | tf_op jit(solution)/shard_map/all_to_all | solution.py:47
  82.7 19.1 %copy-start = (bf16[128,2048]{1,0:T(8,128)(2,1)}, bf16[128,2048]{1,0:T(8,128)(2,1)S(1)}, u32[]{:S(2)}) copy-start(bf16[128,2048]{1,0:T(8,128)(2,1)S(1)} %fusion.9) | copy-start | bytes 1572868
  101.8 142.2 %all-to-all-start = ((bf16[16,96,2048]{2,1,0:T(8,128)(2,1)}), bf16[16,96,2048]{2,1,0:T(8,128)(2,1)}, u32[]{:S(2)}, u32[]{:S(2)}) async-start(bf16[16,96,2048]{2,1,0:T(8,128)(2,1)} %bitcast.77), calls=%async_computation | async-start | bytes 12582912 | tf_op jit(solution)/shard_map/all_to_all | solution.py:79
  263.0 5.0 %copy-start.4 = (f32[512,64]{0,1:T(8,128)S(1)}, f32[512,64]{0,1:T(8,128)}, u32[]{:S(2)}) copy-start(f32[512,64]{0,1:T(8,128)} %param.17) | copy-start | bytes 393220
  263.0 5.0 %copy-start.5 = (f32[512,64]{0,1:T(8,128)S(1)}, f32[512,64]{0,1:T(8,128)}, u32[]{:S(2)}) copy-start(f32[512,64]{0,1:T(8,128)} %param.18) | copy-start | bytes 393220
  263.0 5.0 %copy-start.8 = (f32[512]{0:T(512)S(1)}, f32[512]{0:T(512)}, u32[]{:S(2)}) copy-start(f32[512]{0:T(512)} %param.13) | copy-start | bytes 6148
  263.0 58.0 %copy-start.7 = (f32[128,8]{0,1:T(8,128)S(1)}, f32[128,8]{0,1:T(8,128)}, u32[]{:S(2)}) copy-start(f32[128,8]{0,1:T(8,128)} %param.12) | copy-start | bytes 12292
  263.0 192.9 %all-to-all-start.4 = ((bf16[16,96,2048]{2,1,0:T(8,128)(2,1)}), bf16[16,96,2048]{2,1,0:T(8,128)(2,1)}, u32[]{:S(2)}, u32[]{:S(2)}) async-start(bf16[16,96,2048]{2,1,0:T(8,128)(2,1)} %bitcast.84), calls=%async_computation.4 | async-start | bytes 12582912 | tf_op jit(solution)/shard_map/all_to_all | solution.py:89
  267.9 105.9 %all-gather.4.cloned.1.call-start = ((), (), s32[]{:S(2)}) async-start(), calls=%async_computation.5 | async-start | bytes 1310720 | tf_op jit(solution)/shard_map/all_gather | solution.py:97
  297.9 177.0 %all-gather.6.cloned.1.call-start = ((), (), s32[]{:S(2)}) async-start(), calls=%async_computation.6 | async-start | bytes 1310720 | tf_op jit(solution)/shard_map/all_gather | solution.py:102
  308.3 166.6 %all-gather.8.cloned.1.call-start = ((), (), s32[]{:S(2)}) async-start(), calls=%async_computation.7 | async-start | bytes 1310720 | tf_op jit(solution)/shard_map/all_gather | solution.py:109
  468.4 6.6 %copy-start.1 = (bf16[128,2048]{1,0:T(8,128)(2,1)S(1)}, bf16[128,2048]{1,0:T(8,128)(2,1)}, u32[]{:S(2)}) copy-start(bf16[128,2048]{1,0:T(8,128)(2,1)} %copy-done) | copy-start | bytes 1572868
  468.4 9.9 %copy-start.2 = (bf16[64,2048]{1,0:T(8,128)(2,1)S(1)}, bf16[64,2048]{1,0:T(8,128)(2,1)}, u32[]{:S(2)}) copy-start(bf16[64,2048]{1,0:T(8,128)(2,1)} %all_gather.22) | copy-start | bytes 786436
Sparse Core Ops, SparseCore 0:
  298.0 75.7 all-gather.3
  375.4 37.3 all-gather.5
  414.3 35.7 all-gather.7
where the time goes:
time: 486 us; the launch traced here: 485 us
  waiting for transfers between devices  287 us (59%)
  blocking collectives  79.3 us (16%)
  local copies, waits for them, and re-layouts  42.8 us (9%)
  matrix products  24.1 us (5%)
  starting transfers between devices  19.7 us (4%)
  other arithmetic  19.1 us (4%)
  between operations  13.9 us (3%)
    all_to_all x1, waiting for transfers between devices, on_device(): lax.all_to_all(outbox.reshape(experts, capacity, width), ('fs', 'tp'), sp...  130 us
    all_to_all x1, waiting for transfers between devices, on_device(): lax.all_to_all(finished, ('fs', 'tp'), split_axis=0, concat_axis=0, tiled...  72.7 us
    all_gather x1, waiting for transfers between devices, on_device(): lax.all_gather(held_gate, 'fs', axis=0, tiled=True)  52.7 us
    all_to_all x1, blocking collectives, on_device(): lax.all_to_all(piece_gate[:, None], ('fs', 'tp'), split_axis=0, concat_ax...  31.1 us
    all_gather x1, blocking collectives, on_device(): lax.all_gather(tile_gate, 'tp', axis=1, tiled=True)  29.8 us
    all_to_all x1, waiting for transfers between devices, on_device(): lax.all_to_all(piece_up[:, None], ('fs', 'tp'), split_axis=0, concat_axis...  22.1 us
    dot_general x1, matrix products, expert_rows(): jnp.dot(hidden, w_down, preferred_element_type=jnp.float32)  12.9 us
    gather x1, local copies, waits for them, and re-layouts, on_device(): results = returned.reshape(experts * capacity, width)[target]  12.4 us
  transfers between devices with their start and end apart: 7, of which 5 were waited for; matrix products, arithmetic and copies ran while one was open for 12% of the time, Pallas kernels for 0%

commit v1 on v0

--- a/solution.py
+++ b/solution.py
@@ -86,7 +86,15 @@
     finished = expert_rows(
         arrived.reshape(-1, width), served_gate[0], served_up[0], served_down[0]
     ).reshape(arrived.shape)
-    returned = lax.all_to_all(finished, ("fs", "tp"), split_axis=0, concat_axis=0, tiled=True)
+    ways, here = (lax.axis_size(("fs", "tp")), lax.axis_index(("fs", "tp")))
+    width_2 = finished.shape[0] // ways
+    turned = jnp.roll(finished, -here * width_2, axis=0)
+    got = [lax.slice_in_dim(turned, 0, width_2, axis=0)]
+    for far in range(1, ways):
+        sent = lax.slice_in_dim(turned, far * width_2, (far + 1) * width_2, axis=0)
+        got.append(lax.ppermute(sent, ("fs", "tp"), [(d, (d + far) % ways) for d in range(ways)]))
+    line = jnp.concatenate(got[::-1], axis=0)
+    returned = jnp.roll(line, (here + 1) * got[0].shape[0], axis=0)
     results = returned.reshape(experts * capacity, width)[target]
     routed = jnp.sum(
         results.reshape(rows_dev, picks, width).astype(jnp.float32) * weights[:, :, None], axis=1

time: 486 us -> 517 us (1.064); the launches traced: 485 us -> 508 us
  starting transfers between devices: 19.7 us -> 98.6 us
  waiting for transfers between devices: 287 us -> 215 us
  local copies, waits for them, and re-layouts: 42.8 us -> 51.5 us
  other arithmetic: 19.1 us -> 26.9 us
    ppermute x0 -> x15, starting transfers between devices: none -> 83.7 us  [on_device(): lax.ppermute(sent, ('fs', 'tp'), [(d, (d + far) % ways) for d in range(wa...]
    all_to_all x1 -> x0, waiting for transfers between devices: 72.7 us -> none  [on_device(): lax.all_to_all(finished, ('fs', 'tp'), split_axis=0, concat_axis=0, tiled...]
    ppermute x0 -> x15, waiting for transfers between devices: none -> 53.6 us  [on_device(): lax.ppermute(sent, ('fs', 'tp'), [(d, (d + far) % ways) for d in range(wa...]
    all_gather x1, waiting for transfers between devices: 52.7 us -> 0.01 us  [on_device(): lax.all_gather(held_gate, 'fs', axis=0, tiled=True)]
    concatenate x0 -> x2, other arithmetic: none -> 8.81 us  [the longest x1 4.6 us: on_device(): turned = jnp.roll(finished, -here * width_2, axis=0)]
    unnamed x27 -> x54, local copies, waits for them, and re-layouts: 11.7 us -> 16.8 us
  transfers between devices with their start and end apart: 7 -> 21, of which waited for: 5 -> 10; matrix products, arithmetic and copies ran while one was open for 12% -> 18% of each run, Pallas kernels for 0% -> 0%
where the time goes in v1:
time: 517 us; the launch traced here: 508 us
  waiting for transfers between devices  215 us (42%)
  starting transfers between devices  98.6 us (19%)
  blocking collectives  77.9 us (15%)
  local copies, waits for them, and re-layouts  51.5 us (10%)
  other arithmetic  26.9 us (5%)
  matrix products  24.1 us (5%)
  between operations  14.2 us (3%)
    all_to_all x1, waiting for transfers between devices, on_device(): lax.all_to_all(outbox.reshape(experts, capacity, width), ('fs', 'tp'), sp...  130 us
    ppermute x15, starting transfers between devices, on_device(): lax.ppermute(sent, ('fs', 'tp'), [(d, (d + far) % ways) for d in range(wa...  83.7 us
    ppermute x15, waiting for transfers between devices, on_device(): lax.ppermute(sent, ('fs', 'tp'), [(d, (d + far) % ways) for d in range(wa...  53.6 us
    all_to_all x1, blocking collectives, on_device(): lax.all_to_all(piece_gate[:, None], ('fs', 'tp'), split_axis=0, concat_ax...  31.2 us
    all_gather x1, blocking collectives, on_device(): lax.all_gather(tile_gate, 'tp', axis=1, tiled=True)  29.8 us
    all_to_all x1, waiting for transfers between devices, on_device(): lax.all_to_all(piece_up[:, None], ('fs', 'tp'), split_axis=0, concat_axis...  22.1 us
    unnamed x54, local copies, waits for them, and re-layouts  16.8 us
    dot_general x1, matrix products, expert_rows(): jnp.dot(hidden, w_down, preferred_element_type=jnp.float32)  12.9 us
  transfers between devices with their start and end apart: 21, of which 10 were waited for; matrix products, arithmetic and copies ran while one was open for 18% of the time, Pallas kernels for 0%

profile of v1, /device:TPU:11, one launch (start us, length us, event | category | flops | bytes accessed | tf_op | source)
XLA Modules:
  0.0 507.7 jit_solution(11155190601491619431)
XLA Ops:
  7.2 3.8 fusion.12
  11.0 31.2 %all_to_all.32 = bf16[16,1,512,64]{2,3,1,0:T(8,128)(2,1)S(1)} all-to-all(bf16[16,1,512,64]{2,3,1,0:T(8,128)(2,1)S(1)} %get-tuple-element.52), channel_id=1, replica_groups=mesh['grp'=2,'fs'=4,'tp'=4] {'fs','tp'}, dimensions={0} | all-to-all | bytes 2097152 | tf_op jit(solution)/shard_map/all_to_all | solution.py:45
  42.2 4.9 all-to-all-start.2
  49.9 22.1 %all-to-all-done.2 = bf16[16,1,512,64]{2,3,1,0:T(8,128)(2,1)S(1)} async-done(((bf16[16,1,512,64]{2,3,1,0:T(8,128)(2,1)}), bf16[16,1,512,64]{2,3,1,0:T(8,128)(2,1)S(1)}, u32[]{:S(2)}, u32[]{:S(2)}) %all-to-all-start.2) | async-done | bytes 1048608 | tf_op jit(solution)/shard_map/all_to_all | solution.py:46
  72.0 4.8 all-to-all-start.3
  77.1 4.5 reduce-window.6
  82.7 10.2 %scatter_custom_fusion = bf16[1536,2048]{1,0:T(8,128)(2,1)} fusion(s32[1024]{0:T(1024)S(1)} %bitcast.94, bf16[]{:T(256)} %constant.42.clone.1, bf16[128,2048]{1,0:T(8,128)(2,1)S(1)} %fusion.11), kind=kCustom, calls=%fused_computation.11 | custom fusion | bytes 6815746 | tf_op jit(solution)/shard_map/scatter | solution.py:77
  92.9 8.9 %all-to-all-done.3 = bf16[16,1,64,512]{3,2,1,0:T(8,128)(2,1)} async-done(((bf16[16,1,64,512]{3,2,1,0:T(8,128)(2,1)}), bf16[16,1,64,512]{3,2,1,0:T(8,128)(2,1)}, u32[]{:S(2)}, u32[]{:S(2)}) %all-to-all-start.3) | async-done | bytes 1048608 | tf_op jit(solution)/shard_map/all_to_all | solution.py:47
  101.8 5.0 all-to-all-start
  106.9 29.8 %all_gather.18 = bf16[512,256]{0,1:T(8,128)(2,1)} all-gather(bf16[512,64]{0,1:T(8,128)(2,1)S(1)} %get-tuple-element.50), channel_id=1, replica_groups=mesh['grp'=2,'fs'=4,'tp'=4] {'tp'}, dimensions={1}, use_global_device_ids=true | all-gather | bytes 327680 | tf_op jit(solution)/shard_map/all_gather | solution.py:56
  136.8 10.4 %all_gather.20 = bf16[512,256]{0,1:T(8,128)(2,1)} all-gather(bf16[512,64]{0,1:T(8,128)(2,1)S(1)} %get-tuple-element.51), channel_id=1, replica_groups=mesh['grp'=2,'fs'=4,'tp'=4] {'tp'}, dimensions={1}, use_global_device_ids=true | all-gather | bytes 327680 | tf_op jit(solution)/shard_map/all_gather | solution.py:57
  147.3 6.5 %all_gather.22 = bf16[64,2048]{1,0:T(8,128)(2,1)} all-gather(bf16[64,512]{1,0:T(8,128)(2,1)S(1)} %convert_element_type.63), channel_id=1, replica_groups=mesh['grp'=2,'fs'=4,'tp'=4] {'tp'}, dimensions={1}, use_global_device_ids=true | all-gather | bytes 327680 | tf_op jit(solution)/shard_map/all_gather | solution.py:58
  165.0 129.8 %all-to-all-done = bf16[16,96,2048]{2,1,0:T(8,128)(2,1)} async-done(((bf16[16,96,2048]{2,1,0:T(8,128)(2,1)}), bf16[16,96,2048]{2,1,0:T(8,128)(2,1)}, u32[]{:S(2)}, u32[]{:S(2)}) %all-to-all-start) | async-done | bytes 6291488 | tf_op jit(solution)/shard_map/all_to_all | solution.py:79
  294.8 6.0 %fusion.28 = f32[1536,256]{1,0:T(8,128)} fusion(bf16[1536,2048]{1,0:T(8,128)(2,1)} %bitcast.6, bf16[2048,256]{0,1:T(8,128)(2,1)} %bitcast.88), kind=kOutput, calls=%fused_computation.74 | convolution fusion | flops 1610612736 | bytes 8912896 | tf_op jit(solution)/shard_map/dot_general | solution.py:11
  300.9 12.9 %convolution_convert_fusion = bf16[1536,2048]{1,0:T(8,128)(2,1)} fusion(bf16[256,2048]{1,0:T(8,128)(2,1)} %bitcast.90, bf16[1536,2048]{1,0:T(8,128)(2,1)} %bitcast.6, bf16[2048,256]{0,1:T(8,128)(2,1)} %bitcast.89, f32[1536,256]{1,0:T(8,128)} %fusion.28), kind=kOutput, calls=%fused_computation.8 | convolution fusion | flops 3226730496 | bytes 16252928 | tf_op jit(solution)/shard_map/dot_general | solution.py:14
  313.7 4.6 fusion.2
  333.1 3.9 collective-permute-start.3
  340.5 2.9 collective-permute-start.6
  348.9 8.8 %collective-permute-start.8 = (bf16[1,96,2048]{2,1,0:T(8,128)(2,1)}, bf16[1,96,2048]{2,1,0:T(8,128)(2,1)S(1)}, u32[]{:S(2)}, u32[]{:S(2)}) collective-permute-start(bf16[1,96,2048]{2,1,0:T(8,128)(2,1)} %get-tuple-element.35), channel_id=1, source_target_pairs={{0,7},{1,8},{2,9},{3,10},{4,11},{5,12},{6,13},{7,14},{8,15},{9,0},... | collective-permute-start | bytes 1179656 | tf_op jit(solution)/shard_map/ppermute | solution.py:95
  357.7 6.3 %collective-permute-done.4 = bf16[1,96,2048]{2,1,0:T(8,128)(2,1)S(1)} collective-permute-done((bf16[1,96,2048]{2,1,0:T(8,128)(2,1)}, bf16[1,96,2048]{2,1,0:T(8,128)(2,1)S(1)}, u32[]{:S(2)}, u32[]{:S(2)}) %collective-permute-start.4) | collective-permute-done | bytes 393248 | tf_op jit(solution)/shard_map/ppermute | solution.py:95
  364.0 3.3 collective-permute-start.9
  367.3 6.0 %collective-permute-done.5 = bf16[1,96,2048]{2,1,0:T(8,128)(2,1)S(1)} collective-permute-done((bf16[1,96,2048]{2,1,0:T(8,128)(2,1)}, bf16[1,96,2048]{2,1,0:T(8,128)(2,1)S(1)}, u32[]{:S(2)}, u32[]{:S(2)}) %collective-permute-start.5) | collective-permute-done | bytes 393248 | tf_op jit(solution)/shard_map/ppermute | solution.py:95
  375.4 4.6 collective-permute-done.6
  381.7 19.6 %collective-permute-done.7 = bf16[1,96,2048]{2,1,0:T(8,128)(2,1)S(1)} collective-permute-done((bf16[1,96,2048]{2,1,0:T(8,128)(2,1)}, bf16[1,96,2048]{2,1,0:T(8,128)(2,1)S(1)}, u32[]{:S(2)}, u32[]{:S(2)}) %collective-permute-start.7) | collective-permute-done | bytes 393248 | tf_op jit(solution)/shard_map/ppermute | solution.py:95
  401.4 24.1 %collective-permute-start.12 = (bf16[1,96,2048]{2,1,0:T(8,128)(2,1)S(1)}, bf16[1,96,2048]{2,1,0:T(8,128)(2,1)S(1)}, u32[]{:S(2)}, u32[]{:S(2)}) collective-permute-start(bf16[1,96,2048]{2,1,0:T(8,128)(2,1)S(1)} %copy-done.7), channel_id=1, source_target_pairs={{0,3},{1,4},{2,5},{3,6},{4,7},{5,8},{6,9},{7,10},{8,11},{9,12},{10... | collective-permute-start | bytes 1179656 | tf_op jit(solution)/shard_map/ppermute | solution.py:95
  425.6 31.9 %collective-permute-start.13 = (bf16[1,96,2048]{2,1,0:T(8,128)(2,1)S(1)}, bf16[1,96,2048]{2,1,0:T(8,128)(2,1)S(1)}, u32[]{:S(2)}, u32[]{:S(2)}) collective-permute-start(bf16[1,96,2048]{2,1,0:T(8,128)(2,1)S(1)} %copy-done.6), channel_id=1, source_target_pairs={{0,2},{1,3},{2,4},{3,5},{4,6},{5,7},{6,8},{7,9},{8,10},{9,11},{10,... | collective-permute-start | bytes 1179656 | tf_op jit(solution)/shard_map/ppermute | solution.py:95
  457.8 8.6 %collective-permute-done.13 = bf16[1,96,2048]{2,1,0:T(8,128)(2,1)S(1)} collective-permute-done((bf16[1,96,2048]{2,1,0:T(8,128)(2,1)S(1)}, bf16[1,96,2048]{2,1,0:T(8,128)(2,1)S(1)}, u32[]{:S(2)}, u32[]{:S(2)}) %collective-permute-start.13) | collective-permute-done | bytes 393248 | tf_op jit(solution)/shard_map/ppermute | solution.py:95
  466.4 6.5 %collective-permute-done.14 = bf16[1,96,2048]{2,1,0:T(8,128)(2,1)S(1)} collective-permute-done((bf16[1,96,2048]{2,1,0:T(8,128)(2,1)S(1)}, bf16[1,96,2048]{2,1,0:T(8,128)(2,1)S(1)}, u32[]{:S(2)}, u32[]{:S(2)}) %collective-permute-start.14) | collective-permute-done | bytes 393248 | tf_op jit(solution)/shard_map/ppermute | solution.py:95
  473.9 4.2 fusion.1
  478.2 12.5 %gather_fusion = bf16[1024,2048]{1,0:T(8,128)(2,1)} fusion(bf16[1536,2048]{1,0:T(8,128)(2,1)} %bitcast.77, s32[1024]{0:T(1024)S(1)} %broadcast_clamp_fusion), kind=kCustom, calls=%fused_computation | custom fusion | bytes 8392704 | tf_op jit(solution)/shard_map/gather | solution.py:98
  490.6 6.5 %fusion = f32[128,2048]{1,0:T(8,128)S(1)} fusion(bf16[1024,2048]{1,0:T(8,128)(2,1)} %gather_fusion, f32[128,8]{1,0:T(8,128)S(1)} %copy.61), kind=kLoop, calls=%fused_computation.7 | loop fusion | flops 6029312 | bytes 5246976 | tf_op jit(solution)/shard_map/reduce_sum | solution.py:99
  497.2 3.3 fusion.7
  (114 shorter events, 45.1 us)
Async XLA Ops:
  11.0 65.8 %copy-start.12 = (s32[128,8]{0,1:T(8,128)S(1)}, s32[128,8]{0,1:T(8,128)}, u32[]{:S(2)}) copy-start(s32[128,8]{0,1:T(8,128)} %param.13) | copy-start | bytes 12292
  11.0 71.3 %copy-start.4 = (bf16[128,2048]{1,0:T(8,128)(2,1)S(1)}, bf16[128,2048]{1,0:T(8,128)(2,1)}, u32[]{:S(2)}) copy-start(bf16[128,2048]{1,0:T(8,128)(2,1)} %param.12) | copy-start | bytes 1572868
  42.2 29.8 %all-to-all-start.2 = ((bf16[16,1,512,64]{2,3,1,0:T(8,128)(2,1)}), bf16[16,1,512,64]{2,3,1,0:T(8,128)(2,1)S(1)}, u32[]{:S(2)}, u32[]{:S(2)}) async-start(bf16[16,1,512,64]{2,3,1,0:T(8,128)(2,1)} %get-tuple-element.53), calls=%async_computation.2 | async-start | bytes 2097152 | tf_op jit(solution)/shard_map/all_to_all | solution.py:46
  72.0 29.8 %all-to-all-start.3 = ((bf16[16,1,64,512]{3,2,1,0:T(8,128)(2,1)}), bf16[16,1,64,512]{3,2,1,0:T(8,128)(2,1)}, u32[]{:S(2)}, u32[]{:S(2)}) async-start(bf16[16,1,64,512]{3,2,1,0:T(8,128)(2,1)} %convert_bitcast_fusion), calls=%async_computation.3 | async-start | bytes 2097152 | tf_op jit(solution)/shard_map/all_to_all | solution.py:47
  82.7 19.1 %copy-start.1 = (bf16[128,2048]{1,0:T(8,128)(2,1)}, bf16[128,2048]{1,0:T(8,128)(2,1)S(1)}, u32[]{:S(2)}) copy-start(bf16[128,2048]{1,0:T(8,128)(2,1)S(1)} %fusion.11) | copy-start | bytes 1572868
  101.8 45.4 %copy-start.11 = (f32[64,512]{1,0:T(8,128)S(1)}, f32[64,512]{1,0:T(8,128)}, u32[]{:S(2)}) copy-start(f32[64,512]{1,0:T(8,128)} %param.21) | copy-start | bytes 393220
  101.8 55.6 %copy-start.13 = (f32[128,8]{0,1:T(8,128)S(1)}, f32[128,8]{0,1:T(8,128)}, u32[]{:S(2)}) copy-start(f32[128,8]{0,1:T(8,128)} %param.14) | copy-start | bytes 12292
  101.8 193.0 %all-to-all-start = ((bf16[16,96,2048]{2,1,0:T(8,128)(2,1)}), bf16[16,96,2048]{2,1,0:T(8,128)(2,1)}, u32[]{:S(2)}, u32[]{:S(2)}) async-start(bf16[16,96,2048]{2,1,0:T(8,128)(2,1)} %bitcast.78), calls=%async_computation | async-start | bytes 12582912 | tf_op jit(solution)/shard_map/all_to_all | solution.py:79
  106.8 216.9 %all-gather.4.cloned.1.call-start = ((), (), s32[]{:S(2)}) async-start(), calls=%async_computation.4 | async-start | bytes 1310720 | tf_op jit(solution)/shard_map/all_gather | solution.py:105
  136.8 360.4 %all-gather.6.cloned.1.call-start = ((), (), s32[]{:S(2)}) async-start(), calls=%async_computation.5 | async-start | bytes 1310720 | tf_op jit(solution)/shard_map/all_gather | solution.py:110
  147.2 350.0 %all-gather.8.cloned.1.call-start = ((), (), s32[]{:S(2)}) async-start(), calls=%async_computation.6 | async-start | bytes 1310720 | tf_op jit(solution)/shard_map/all_gather | solution.py:117
  323.6 14.4 %collective-permute-start = (bf16[1,96,2048]{2,1,0:T(8,128)(2,1)}, bf16[1,96,2048]{2,1,0:T(8,128)(2,1)}, u32[]{:S(2)}, u32[]{:S(2)}) collective-permute-start(bf16[1,96,2048]{2,1,0:T(8,128)(2,1)} %get-tuple-element.43), channel_id=1, source_target_pairs={{0,15},{1,0},{2,1},{3,2},{4,3},{5,4},{6,5},{7,6},{8,7},{9,8},{10,9... | collective-permute-start | bytes 1179656 | tf_op jit(solution)/shard_map/ppermute | solution.py:95
  323.7 16.9 %collective-permute-start.1 = (bf16[1,96,2048]{2,1,0:T(8,128)(2,1)}, bf16[1,96,2048]{2,1,0:T(8,128)(2,1)}, u32[]{:S(2)}, u32[]{:S(2)}) collective-permute-start(bf16[1,96,2048]{2,1,0:T(8,128)(2,1)} %get-tuple-element.42), channel_id=1, source_target_pairs={{0,14},{1,15},{2,0},{3,1},{4,2},{5,3},{6,4},{7,5},{8,6},{9,7},{10,... | collective-permute-start | bytes 1179656 | tf_op jit(solution)/shard_map/ppermute | solution.py:95
  330.2 95.3 %copy-start.6 = (bf16[1,96,2048]{2,1,0:T(8,128)(2,1)S(1)}, bf16[1,96,2048]{2,1,0:T(8,128)(2,1)}, u32[]{:S(2)}) copy-start(bf16[1,96,2048]{2,1,0:T(8,128)(2,1)} %get-tuple-element.30) | copy-start | bytes 1179652
  330.2 127.3 %copy-start.5 = (bf16[1,96,2048]{2,1,0:T(8,128)(2,1)S(1)}, bf16[1,96,2048]{2,1,0:T(8,128)(2,1)}, u32[]{:S(2)}) copy-start(bf16[1,96,2048]{2,1,0:T(8,128)(2,1)} %get-tuple-element.29) | copy-start | bytes 1179652
  331.6 48.5 %copy-start.8 = (bf16[1,96,2048]{2,1,0:T(8,128)(2,1)S(1)}, bf16[1,96,2048]{2,1,0:T(8,128)(2,1)}, u32[]{:S(2)}) copy-start(bf16[1,96,2048]{2,1,0:T(8,128)(2,1)} %get-tuple-element.32) | copy-start | bytes 1179652
  331.6 69.8 %copy-start.7 = (bf16[1,96,2048]{2,1,0:T(8,128)(2,1)S(1)}, bf16[1,96,2048]{2,1,0:T(8,128)(2,1)}, u32[]{:S(2)}) copy-start(bf16[1,96,2048]{2,1,0:T(8,128)(2,1)} %get-tuple-element.31) | copy-start | bytes 1179652
  333.1 13.3 %collective-permute-start.2 = (bf16[1,96,2048]{2,1,0:T(8,128)(2,1)}, bf16[1,96,2048]{2,1,0:T(8,128)(2,1)S(1)}, u32[]{:S(2)}, u32[]{:S(2)}) collective-permute-start(bf16[1,96,2048]{2,1,0:T(8,128)(2,1)} %get-tuple-element.41), channel_id=1, source_target_pairs={{0,13},{1,14},{2,15},{3,0},{4,1},{5,2},{6,3},{7,4},{8,5},{9,6},{10... | collective-permute-start | bytes 1179656 | tf_op jit(solution)/shard_map/ppermute | solution.py:95
  333.1 15.8 %collective-permute-start.3 = (bf16[1,96,2048]{2,1,0:T(8,128)(2,1)}, bf16[1,96,2048]{2,1,0:T(8,128)(2,1)S(1)}, u32[]{:S(2)}, u32[]{:S(2)}) collective-permute-start(bf16[1,96,2048]{2,1,0:T(8,128)(2,1)} %get-tuple-element.40), channel_id=1, source_target_pairs={{0,12},{1,13},{2,14},{3,15},{4,0},{5,1},{6,2},{7,3},{8,4},{9,5},{1... | collective-permute-start | bytes 1179656 | tf_op jit(solution)/shard_map/ppermute | solution.py:95
  337.0 27.0 %collective-permute-start.4 = (bf16[1,96,2048]{2,1,0:T(8,128)(2,1)}, bf16[1,96,2048]{2,1,0:T(8,128)(2,1)S(1)}, u32[]{:S(2)}, u32[]{:S(2)}) collective-permute-start(bf16[1,96,2048]{2,1,0:T(8,128)(2,1)} %get-tuple-element.39), channel_id=1, source_target_pairs={{0,11},{1,12},{2,13},{3,14},{4,15},{5,0},{6,1},{7,2},{8,3},{9,4},{... | collective-permute-start | bytes 1179656 | tf_op jit(solution)/shard_map/ppermute | solution.py:95
  338.0 35.3 %collective-permute-start.5 = (bf16[1,96,2048]{2,1,0:T(8,128)(2,1)}, bf16[1,96,2048]{2,1,0:T(8,128)(2,1)S(1)}, u32[]{:S(2)}, u32[]{:S(2)}) collective-permute-start(bf16[1,96,2048]{2,1,0:T(8,128)(2,1)} %get-tuple-element.38), channel_id=1, source_target_pairs={{0,10},{1,11},{2,12},{3,13},{4,14},{5,15},{6,0},{7,1},{8,2},{9,3},... | collective-permute-start | bytes 1179656 | tf_op jit(solution)/shard_map/ppermute | solution.py:95
  340.5 39.5 %collective-permute-start.6 = (bf16[1,96,2048]{2,1,0:T(8,128)(2,1)}, bf16[1,96,2048]{2,1,0:T(8,128)(2,1)S(1)}, u32[]{:S(2)}, u32[]{:S(2)}) collective-permute-start(bf16[1,96,2048]{2,1,0:T(8,128)(2,1)} %get-tuple-element.37), channel_id=1, source_target_pairs={{0,9},{1,10},{2,11},{3,12},{4,13},{5,14},{6,15},{7,0},{8,1},{9,2},... | collective-permute-start | bytes 1179656 | tf_op jit(solution)/shard_map/ppermute | solution.py:95
  346.4 55.0 %collective-permute-start.7 = (bf16[1,96,2048]{2,1,0:T(8,128)(2,1)}, bf16[1,96,2048]{2,1,0:T(8,128)(2,1)S(1)}, u32[]{:S(2)}, u32[]{:S(2)}) collective-permute-start(bf16[1,96,2048]{2,1,0:T(8,128)(2,1)} %get-tuple-element.36), channel_id=1, source_target_pairs={{0,8},{1,9},{2,10},{3,11},{4,12},{5,13},{6,14},{7,15},{8,0},{9,1},... | collective-permute-start | bytes 1179656 | tf_op jit(solution)/shard_map/ppermute | solution.py:95
  348.9 76.6 %collective-permute-start.8 = (bf16[1,96,2048]{2,1,0:T(8,128)(2,1)}, bf16[1,96,2048]{2,1,0:T(8,128)(2,1)S(1)}, u32[]{:S(2)}, u32[]{:S(2)}) collective-permute-start(bf16[1,96,2048]{2,1,0:T(8,128)(2,1)} %get-tuple-element.35), channel_id=1, source_target_pairs={{0,7},{1,8},{2,9},{3,10},{4,11},{5,12},{6,13},{7,14},{8,15},{9,0},... | collective-permute-start | bytes 1179656 | tf_op jit(solution)/shard_map/ppermute | solution.py:95
  364.0 93.5 %collective-permute-start.9 = (bf16[1,96,2048]{2,1,0:T(8,128)(2,1)}, bf16[1,96,2048]{2,1,0:T(8,128)(2,1)S(1)}, u32[]{:S(2)}, u32[]{:S(2)}) collective-permute-start(bf16[1,96,2048]{2,1,0:T(8,128)(2,1)} %get-tuple-element.34), channel_id=1, source_target_pairs={{0,6},{1,7},{2,8},{3,9},{4,10},{5,11},{6,12},{7,13},{8,14},{9,15},... | collective-permute-start | bytes 1179656 | tf_op jit(solution)/shard_map/ppermute | solution.py:95
  373.3 84.4 %collective-permute-start.10 = (bf16[1,96,2048]{2,1,0:T(8,128)(2,1)}, bf16[1,96,2048]{2,1,0:T(8,128)(2,1)S(1)}, u32[]{:S(2)}, u32[]{:S(2)}) collective-permute-start(bf16[1,96,2048]{2,1,0:T(8,128)(2,1)} %get-tuple-element.33), channel_id=1, source_target_pairs={{0,5},{1,6},{2,7},{3,8},{4,9},{5,10},{6,11},{7,12},{8,13},{9,14},{... | collective-permute-start | bytes 1179656 | tf_op jit(solution)/shard_map/ppermute | solution.py:95
  380.1 77.6 %collective-permute-start.11 = (bf16[1,96,2048]{2,1,0:T(8,128)(2,1)S(1)}, bf16[1,96,2048]{2,1,0:T(8,128)(2,1)S(1)}, u32[]{:S(2)}, u32[]{:S(2)}) collective-permute-start(bf16[1,96,2048]{2,1,0:T(8,128)(2,1)S(1)} %copy-done.8), channel_id=1, source_target_pairs={{0,4},{1,5},{2,6},{3,7},{4,8},{5,9},{6,10},{7,11},{8,12},{9,13},{1... | collective-permute-start | bytes 1179656 | tf_op jit(solution)/shard_map/ppermute | solution.py:95
  401.4 56.3 %collective-permute-start.12 = (bf16[1,96,2048]{2,1,0:T(8,128)(2,1)S(1)}, bf16[1,96,2048]{2,1,0:T(8,128)(2,1)S(1)}, u32[]{:S(2)}, u32[]{:S(2)}) collective-permute-start(bf16[1,96,2048]{2,1,0:T(8,128)(2,1)S(1)} %copy-done.7), channel_id=1, source_target_pairs={{0,3},{1,4},{2,5},{3,6},{4,7},{5,8},{6,9},{7,10},{8,11},{9,12},{10... | collective-permute-start | bytes 1179656 | tf_op jit(solution)/shard_map/ppermute | solution.py:95
  425.6 40.8 %collective-permute-start.13 = (bf16[1,96,2048]{2,1,0:T(8,128)(2,1)S(1)}, bf16[1,96,2048]{2,1,0:T(8,128)(2,1)S(1)}, u32[]{:S(2)}, u32[]{:S(2)}) collective-permute-start(bf16[1,96,2048]{2,1,0:T(8,128)(2,1)S(1)} %copy-done.6), channel_id=1, source_target_pairs={{0,2},{1,3},{2,4},{3,5},{4,6},{5,7},{6,8},{7,9},{8,10},{9,11},{10,... | collective-permute-start | bytes 1179656 | tf_op jit(solution)/shard_map/ppermute | solution.py:95
  457.5 15.4 %collective-permute-start.14 = (bf16[1,96,2048]{2,1,0:T(8,128)(2,1)S(1)}, bf16[1,96,2048]{2,1,0:T(8,128)(2,1)S(1)}, u32[]{:S(2)}, u32[]{:S(2)}) collective-permute-start(bf16[1,96,2048]{2,1,0:T(8,128)(2,1)S(1)} %copy-done.5), channel_id=1, source_target_pairs={{0,1},{1,2},{2,3},{3,4},{4,5},{5,6},{6,7},{7,8},{8,9},{9,10},{10,1... | collective-permute-start | bytes 1179656 | tf_op jit(solution)/shard_map/ppermute | solution.py:95
  478.2 19.1 %copy-start.2 = (bf16[128,2048]{1,0:T(8,128)(2,1)S(1)}, bf16[128,2048]{1,0:T(8,128)(2,1)}, u32[]{:S(2)}) copy-start(bf16[128,2048]{1,0:T(8,128)(2,1)} %copy-done.1) | copy-start | bytes 1572868
  490.6 9.9 %copy-start.3 = (bf16[64,2048]{1,0:T(8,128)(2,1)S(1)}, bf16[64,2048]{1,0:T(8,128)(2,1)}, u32[]{:S(2)}) copy-start(bf16[64,2048]{1,0:T(8,128)(2,1)} %all_gather.22) | copy-start | bytes 786436
  (4 other events, 17.8 us)
Sparse Core Ops, SparseCore 0:
  136.9 75.7 all-gather.3
  214.2 37.3 all-gather.5
  253.2 35.7 all-gather.7
